TPU v7x, 32 devices: a whole 2x2x4 slice. The times are simulated.
32 devices in a mesh: kv: 16 (over z, y, x), tp: 2 (over core).
Axes of the slice: x: 2, y: 2, z: 4, core: 2. Of those that a mesh axis runs over, the one named last changes fastest.
Arguments:
- tokens: bfloat16 [64, 4096], P(None, 'kv'), may hold values from -160 to 160
- norm_gain: float32 [4096], P('kv'), may hold values from 0.1 to 1.9
- w_query: bfloat16 [4096, 2048], P('kv', 'tp'), may hold values from -0.09375 to 0.09375
- w_key: bfloat16 [4096, 2048], P('kv', 'tp'), may hold values from -0.5 to 0.5
- w_value: bfloat16 [4096, 2048], P('kv', 'tp'), may hold values from -0.09375 to 0.09375
- w_out: bfloat16 [2048, 4096], P('tp', 'kv'), may hold values from -0.125 to 0.125
- lambdas: float32 [16], P('tp'), may hold values from 0.3 to 0.8
- sub_gain: float32 [128], replicated, may hold values from 0.1 to 1.9
- key_cache: bfloat16 [4, 16, 8192, 128], P(None, 'tp', 'kv'), may hold values from -512 to 512
- value_cache: bfloat16 [4, 16, 8192, 128], P(None, 'tp', 'kv'), may hold values from -6 to 6
- prior: int32 [4], replicated, may hold values from 6144 to 8160
- accepted: int32 [4], replicated, may hold values from 1 to 16
- parent: int32 [4, 16], replicated, may hold values from -1 to 14, as said below
Outputs:
- mixed: bfloat16 [64, 4096], P('tp', 'kv')
- key_out: bfloat16 [4, 16, 8192, 128], P(None, 'tp', 'kv')
- value_out: bfloat16 [4, 16, 8192, 128], P(None, 'tp', 'kv')
Inputs may be any that keep to these rules, and one draw needn't show every extreme that they name: parent[s, 0] is -1, and 0 <= parent[s, j] < j for j >= 1.
All inputs are finite; a program needn't handle non-finite values.
Results may differ from a plain program's by a relative error of at most 0.015.
The roundings to bfloat16 on the way count: a program that leaves them out, or rounds other values in their place, can miss the bound.
Values may be sent and summed in bfloat16 or wider, within the bound.
No kernel may reach another device: no remote copies, remote signals or barrier semaphores. Data moves between devices by JAX's collectives and lax.ppermute only.
A program may use at most 64 MiB of HBM per device.

v0:
```python
import jax
import jax.numpy as jnp
from jax import lax
from jax.sharding import PartitionSpec as P

D = 4096


epsilon = 1e-06
masked_score = -1e30
head_scale = 0.8


def merged_2(array, axis, combine):
    everything = jax.tree.map(lambda part: lax.all_gather(part, axis), array)
    initial = jax.tree.map(lambda part: part[0], everything)

    def step(k, so_far):
        return combine(so_far, jax.tree.map(lambda part: part[k], everything))

    return lax.fori_loop(1, lax.axis_size(axis), step, initial)


def ancestors(parent):
    prop_count = parent.shape[1]
    identity = jnp.eye(prop_count, dtype=jnp.float32)
    parent_hot = (
        parent[:, :, None] == jnp.arange(prop_count, dtype=jnp.int32)[None, None, :]
    ).astype(jnp.float32)

    def extend(depth_step, ancestry):
        return identity[None] + jnp.einsum(
            "sjm,smi->sji", parent_hot, ancestry, precision=lax.Precision.HIGHEST
        )

    return lax.fori_loop(0, prop_count, extend, jnp.broadcast_to(identity, parent_hot.shape))


def combine(earlier, later):
    max_early, totals_early, summed_early = earlier
    max_late, totals_late, summed_late = later
    maximum = jnp.maximum(max_early, max_late)
    factor_early = jnp.exp(max_early - maximum)
    factor_late = jnp.exp(max_late - maximum)
    totals = totals_early * factor_early + totals_late * factor_late
    summed = summed_early * factor_early[..., None] + summed_late * factor_late[..., None]
    return (maximum, totals, summed)


def partial_attend(queries, keys, values, allowed):
    seq_count, head_count, length = (keys.shape[0], keys.shape[1], keys.shape[2])
    head_dim = queries.shape[-1]
    halves = keys.reshape(seq_count, head_count, length, 2, head_dim)
    scores = jnp.einsum(
        "sjhmd,shpmd->mshjp", queries, halves, preferred_element_type=jnp.float32
    ) * head_dim ** (-0.5)
    visible = allowed[None, :, None, :, :]
    maximum = jnp.max(jnp.where(visible, scores, masked_score), axis=-1)
    weight = jnp.where(visible, jnp.exp(scores - maximum[..., None]), 0.0)
    totals = jnp.sum(weight, axis=-1)
    summed = jnp.einsum(
        "mshjp,shpc->mshjc", weight.astype(jnp.bfloat16), values, preferred_element_type=jnp.float32
    )
    return (maximum, totals, summed)


def body(
    tokens,
    norm_gain,
    w_query,
    w_key,
    w_value,
    w_out,
    lambdas,
    sub_gain,
    key_cache,
    value_cache,
    prior,
    accepted,
    parent,
):
    seq_count, prop_count = parent.shape
    head_count = lambdas.shape[0]
    head_dim = w_query.shape[1] // (2 * head_count)
    value_dim = sub_gain.shape[0]
    length = key_cache.shape[2]
    as_float = tokens.astype(jnp.float32)
    row_squares = jnp.sum(as_float * as_float, axis=1)
    normed = (as_float * norm_gain[None, :]).astype(jnp.bfloat16)
    part_query = jnp.dot(normed, w_query, preferred_element_type=jnp.float32)
    part_key = jnp.dot(normed, w_key, preferred_element_type=jnp.float32)
    part_value = jnp.dot(normed, w_value, preferred_element_type=jnp.float32)
    sum_query, sum_key, sum_value, sum_squares = lax.psum(
        (part_query, part_key, part_value, row_squares), "kv"
    )
    row_scale = lax.rsqrt(sum_squares / D + epsilon)[:, None]
    queries = (row_scale * sum_query).astype(jnp.bfloat16)
    new_key = (row_scale * sum_key).astype(jnp.bfloat16)
    new_value = (row_scale * sum_value).astype(jnp.bfloat16)
    queries = queries.reshape(seq_count, prop_count, head_count, 2, head_dim)
    new_key = new_key.reshape(seq_count, prop_count, head_count, 2 * head_dim).transpose(0, 2, 1, 3)
    new_value = new_value.reshape(seq_count, prop_count, head_count, value_dim).transpose(
        0, 2, 1, 3
    )
    valid_end = prior + accepted
    positions = lax.axis_index("kv") * length + jnp.arange(length, dtype=jnp.int32)
    offset_in = positions[None, :] - valid_end[:, None]
    one_hot = offset_in[:, :, None] == jnp.arange(prop_count, dtype=jnp.int32)[None, None, :]
    inside = (offset_in >= 0) & (offset_in < prop_count)
    hot_rows = one_hot.astype(jnp.bfloat16)
    placed_key = jnp.einsum(
        "spj,shjc->shpc", hot_rows, new_key, preferred_element_type=jnp.float32
    ).astype(jnp.bfloat16)
    placed_value = jnp.einsum(
        "spj,shjc->shpc", hot_rows, new_value, preferred_element_type=jnp.float32
    ).astype(jnp.bfloat16)
    key_out = jnp.where(inside[:, None, :, None], placed_key, key_cache)
    value_out = jnp.where(inside[:, None, :, None], placed_value, value_cache)
    ancestry = ancestors(parent)
    settled = offset_in < 0
    allowed = jnp.broadcast_to(settled[:, None, :], (seq_count, prop_count, length))
    shard_keys, shard_values = (key_cache, value_cache)
    local_terms = partial_attend(queries, shard_keys, shard_values, allowed)
    merged = merged_2(local_terms, "kv", combine)
    own_terms = partial_attend(queries, new_key, new_value, ancestry > 0.5)
    merged = combine(merged, own_terms)
    maximum, totals, summed = merged
    head_out = (
        summed[0] / totals[0][..., None]
        - lambdas[None, :, None, None] * summed[1] / totals[1][..., None]
    )
    mean_square = jnp.mean(head_out * head_out, axis=-1, keepdims=True)
    attended = (head_out * lax.rsqrt(mean_square + epsilon) * sub_gain * head_scale).astype(
        jnp.bfloat16
    )
    attended = attended.transpose(0, 2, 1, 3).reshape(
        seq_count * prop_count, head_count * value_dim
    )
    partial_value = jnp.dot(attended, w_out, preferred_element_type=jnp.float32).astype(
        jnp.bfloat16
    )
    mixed = lax.psum_scatter(
        partial_value.astype(jnp.float32).astype(jnp.bfloat16),
        "tp",
        scatter_dimension=0,
        tiled=True,
    )
    return (mixed, key_out, value_out)


def solution(mesh):
    return jax.shard_map(
        body,
        mesh=mesh,
        in_specs=(
            P(None, "kv"),
            P("kv"),
            P("kv", "tp"),
            P("kv", "tp"),
            P("kv", "tp"),
            P("tp", "kv"),
            P("tp"),
            P(),
            P(None, "tp", "kv", None),
            P(None, "tp", "kv", None),
            P(),
            P(),
            P(),
        ),
        out_specs=(P("tp", "kv"), P(None, "tp", "kv", None), P(None, "tp", "kv", None)),
        check_vma=False,
    )
```

profile of v0, /device:TPU:0, one launch (start us, length us, event | category | flops | bytes accessed | tf_op | source)
XLA Modules:
  0.0 306.8 jit_solution(12659445061941012506)
XLA Ops:
  7.2 1.0 copy-done
  8.2 1.7 fusion.51
  9.9 2.0 fusion.53
  11.9 2.0 fusion.55
  14.0 6.2 %copy.56 = bf16[4,8,512,128]{2,3,1,0:T(8,128)(2,1)} copy(bf16[4,8,512,128]{3,2,1,0:T(8,128)(2,1)} %param.25) | data formatting | bytes 8388608 | tf_op args[8]
  20.2 0.1 fusion.45
  20.3 43.6 %psum.28 = f32[64]{0:T(128)S(1)} all-reduce(f32[64]{0:T(128)S(1)} %fusion.45), channel_id=1, replica_groups=mesh['kv'=16,'tp'=2] {'kv'}, use_global_device_ids=true, to_apply=%region_1.0 | all-reduce | flops 64 | bytes 512 | tf_op jit(solution)/shard_map/psum | solution.py:93
  63.9 0.1 fusion.57
  64.0 64.9 %all-reduce.3.cloned.1.call-done = (f32[64,1024]{1,0:T(8,128)}, f32[64,1024]{1,0:T(8,128)}, f32[64,1024]{1,0:T(8,128)}) async-done(((f32[64,1024]{1,0:T(8,128)}, f32[64,1024]{1,0:T(8,128)}, f32[64,1024]{1,0:T(8,128)}), (f32[64,1024]{1,0:T(8,128)}, f32[64,1024]{1,0:T(8,128)}, f32[64,1024]{1,0:T(8,128)})) %all-reduce.3.cloned.1.call-update) | async-done | bytes 786448 | tf_op jit(solution)/shard_map/psum | solution.py:93
  128.9 1.2 fusion.34
  130.1 0.2 reshape.105
  130.3 3.2 %select_reduce_fusion = (f32[2,4,8,16]{3,2,1,0:T(8,128)S(1)}, f32[2,4,8,16,512]{4,3,2,1,0:T(8,128)S(1)}) fusion(pred[4,512]{1,0:T(4,128)(4,1)S(1)} %get-tuple-element.286, bf16[4,8,512,2,64]{2,4,3,1,0:T(8,128)(2,1)} %bitcast.109, bf16[4,16,8,2,64]{4,3,2,1,0:T(2,128)(2,1)S(1)} %reshape.105), kind=kOutput, calls=%fused_computation.25 | convolution fusion | flops 68680704 | bytes 6428672 | tf_op jit(solution)/shard_map/sjhmd,shpmd->mshjp/dot_general | solution.py:54
  133.5 0.7 fusion.15
  134.2 1.6 fusion.19
  135.8 6.2 %copy.74 = bf16[4,8,512,128]{2,3,1,0:T(8,128)(2,1)} copy(bf16[4,8,512,128]{3,2,1,0:T(8,128)(2,1)} %param.26) | data formatting | bytes 8388608 | tf_op args[9]
  142.0 4.4 %while.31 = (s32[]{:T(128)}, f32[4,16,16]{2,1,0:T(8,128)S(1)}, s32[4,16]{1,0:T(4,128)S(1)}, s32[]{:T(128)}) while((s32[]{:T(128)}, f32[4,16,16]{2,1,0:T(8,128)S(1)}, s32[4,16]{1,0:T(4,128)S(1)}, s32[]{:T(128)}) %tuple.94), condition=%wide.region_8.9_spmd.clone, body=%wide.region_7.8_spmd.clone.sunk | while | flops 200194 | bytes 18741 | solution.py:36
  142.1 0.2 convolution_add_fusion.2
  142.3 0.2 convolution_add_fusion.2
  142.6 0.2 convolution_add_fusion.2
  142.9 0.2 convolution_add_fusion.2
  143.2 0.2 convolution_add_fusion.2
  143.5 0.2 convolution_add_fusion.2
  143.7 0.2 convolution_add_fusion.2
  144.0 0.2 convolution_add_fusion.2
  144.3 0.2 convolution_add_fusion.2
  144.6 0.2 convolution_add_fusion.2
  144.8 0.2 convolution_add_fusion.2
  145.1 0.2 convolution_add_fusion.2
  145.4 0.2 convolution_add_fusion.2
  145.7 0.2 convolution_add_fusion.2
  145.9 0.2 convolution_add_fusion.2
  146.2 0.2 convolution_add_fusion.2
  146.5 0.1 copy.62
  146.7 46.1 %all-gather.1 = f32[32,4,8,16]{3,2,1,0:T(8,128)S(1)} all-gather(f32[2,4,8,16]{3,2,1,0:T(8,128)S(1)} %get-tuple-element.280), channel_id=3, replica_groups=mesh['kv'=16,'tp'=2] {'kv'}, dimensions={0}, use_global_device_ids=true | all-gather | bytes 69632 | tf_op jit(solution)/shard_map/all_gather | solution.py:15
  192.8 43.3 %all-gather = f32[32,4,8,16]{3,2,1,0:T(8,128)S(1)} all-gather(f32[2,4,8,16]{3,2,1,0:T(8,128)S(1)} %get-tuple-element.292), channel_id=2, replica_groups=mesh['kv'=16,'tp'=2] {'kv'}, dimensions={0}, use_global_device_ids=true | all-gather | bytes 69632 | tf_op jit(solution)/shard_map/all_gather | solution.py:15
  236.1 0.1 reshape.108
  236.3 0.3 select_reduce_fusion.1
  236.6 0.2 fusion.24
  236.8 5.5 %bitcast_select_fusion.1 = bf16[4,8,512,128]{2,3,1,0:T(8,128)(2,1)} fusion(bf16[4,8,512,128]{2,3,1,0:T(8,128)(2,1)} %copy.56, pred[4,512]{1,0:T(4,128)(4,1)S(1)} %get-tuple-element.285, s32[4,512]{1,0:T(4,128)S(1)} %broadcast_subtract_fusion, bf16[4,16,8,128]{3,2,1,0:T(8,128)(2,1)S(1)} %bitcast.111), kind=kOutput, calls=%fused_computation.21 | convolution fusion | flops 71335936 | bytes 8529920 | tf_op jit(solution)/shard_map/spj,shjc->shpc/dot_general | solution.py:111
  242.3 14.2 %all-gather.5.cloned.1.call-done = f32[32,4,8,16,128]{4,3,0,2,1:T(8,128)} async-done(((f32[2,4,8,16,128]{4,3,0,2,1:T(8,128)}), f32[32,4,8,16,128]{4,3,0,2,1:T(8,128)}) %all-gather.5.cloned.1.call-update) | async-done | bytes 8388624 | tf_op jit(solution)/shard_map/all_gather | solution.py:15
  256.6 1.1 slice.33
  257.7 22.7 %while.30 = (s32[]{:T(128)}, f32[2,4,8,16]{3,2,1,0:T(8,128)S(1)}, f32[2,4,8,16]{3,2,1,0:T(8,128)S(1)}, f32[2,4,8,16,128]{4,3,2,1,0:T(8,128)S(1)}, f32[16,2,4,8,1...) while((s32[]{:T(128)}, f32[2,4,8,16]{3,2,1,0:T(8,128)S(1)}, ...), condition=%wide.region_6.7_spmd, body=%wide.region_5.6_spmd.sunk | while | flops 399365 | bytes 1613975 | solution.py:21
  257.8 1.4 fusion.74
  259.3 1.4 fusion.74
  260.8 1.4 fusion.74
  262.3 1.4 fusion.74
  263.8 1.4 fusion.74
  265.3 1.4 fusion.74
  266.8 1.4 fusion.74
  268.3 1.4 fusion.74
  269.9 1.4 fusion.74
  271.4 1.4 fusion.74
  272.9 1.4 fusion.74
  274.4 1.4 fusion.74
  275.9 1.4 fusion.74
  277.4 1.4 fusion.74
  278.9 1.4 fusion.74
  280.5 0.5 fusion.18
  281.1 0.3 multiply_reduce_fusion
  281.4 0.1 fusion.35
  281.6 0.8 convolution_convert_fusion
  282.5 5.4 %bitcast_select_fusion = bf16[4,8,512,128]{2,3,1,0:T(8,128)(2,1)} fusion(bf16[4,8,512,128]{2,3,1,0:T(8,128)(2,1)} %copy.74, pred[4,512]{1,0:T(4,128)(4,1)S(1)} %get-tuple-element.285, bf16[4,16,8,128]{3,2,1,0:T(8,128)(2,1)S(1)} %bitcast.116, s32[4,512]{1,0:T(4,128)S(1)} %broadcast_subtract_fusion), kind=kOutput, calls=%fused_computation.20 | convolution fusion | flops 71335936 | bytes 8529920 | tf_op jit(solution)/shard_map/spj,shjc->shpc/dot_general | solution.py:114
  287.9 6.2 %copy.75 = bf16[4,8,512,128]{3,2,1,0:T(8,128)(2,1)} copy(bf16[4,8,512,128]{2,3,1,0:T(8,128)(2,1)} %bitcast_select_fusion.1) | data formatting | bytes 8388608
  294.1 6.2 %copy.76 = bf16[4,8,512,128]{3,2,1,0:T(8,128)(2,1)} copy(bf16[4,8,512,128]{2,3,1,0:T(8,128)(2,1)} %bitcast_select_fusion) | data formatting | bytes 8388608
  (90 shorter events, 1.3 us)
Async XLA Ops:
  7.2 1.0 copy-start
  7.2 121.7 %all-reduce.3.cloned.1.call-start = ((), (), s32[]{:S(2)}) async-start(), calls=%async_computation.3 | async-start | bytes 1572864 | tf_op jit(solution)/shard_map/psum | solution.py:93
  13.9 242.7 %all-gather.5.cloned.1.call-start = ((), (), s32[]{:S(2)}) async-start(), calls=%async_computation.2 | async-start | bytes 8912896 | tf_op jit(solution)/shard_map/all_gather | solution.py:15
  13.9 6.2 %copy-start.7 = (s32[4]{0:T(128)S(1)}, s32[4]{0:T(128)}, u32[]{:S(2)}) copy-start(s32[4]{0:T(128)} %param.27) | copy-start | bytes 52
  13.9 6.2 %copy-start.8 = (s32[4]{0:T(128)S(1)}, s32[4]{0:T(128)}, u32[]{:S(2)}) copy-start(s32[4]{0:T(128)} %param.28) | copy-start | bytes 52
  14.0 6.2 %copy-start.2 = (bf16[64,256]{1,0:T(8,128)(2,1)S(1)}, bf16[64,256]{1,0:T(8,128)(2,1)}, u32[]{:S(2)}) copy-start(bf16[64,256]{1,0:T(8,128)(2,1)} %param.17) | copy-start | bytes 98308
  130.3 3.9 %copy-start.1 = (bf16[4,8,512,128]{3,2,1,0:T(8,128)(2,1)S(1)}, bf16[4,8,512,128]{3,2,1,0:T(8,128)(2,1)}, u32[]{:S(2)}) copy-start(bf16[4,8,512,128]{3,2,1,0:T(8,128)(2,1)} %param.26) | copy-start | bytes 12582916
  135.7 164.5 %reduce-scatter.2.cloned.1.call-start = ((), (), s32[]{:S(2)}) async-start(), calls=%async_computation.1 | async-start | bytes 49152 | tf_op jit(solution)/shard_map/reduce_scatter | solution.py:142
  135.8 6.2 %copy-start.4 = (s32[4,16]{1,0:T(4,128)S(1)}, s32[4,16]{1,0:T(4,128)}, u32[]{:S(2)}) copy-start(s32[4,16]{1,0:T(4,128)} %param.29) | copy-start | bytes 772
  280.4 0.7 copy-start.6
  280.4 1.0 copy-start.5
  280.4 1.2 copy-start.3
Sparse Core Ops, SparseCore 0:
  14.2 114.5 all-reduce.2
  135.9 120.6 all-gather.4
  282.6 8.9 reduce-scatter.1
where the time goes:
time: 309 us; the launch traced here: 307 us
  blocking collectives  133 us (43%)
  waiting for transfers between devices  79.2 us (26%)
  local copies, waits for them, and re-layouts  27.6 us (9%)
  matrix products  26.5 us (9%)
  other arithmetic  25.2 us (8%)
  between operations  14 us (5%)
    all_gather x2, blocking collectives, merged_2(): everything = jax.tree.map(lambda part: lax.all_gather(part, axis), array)  89.4 us
    psum x1, waiting for transfers between devices, body(): lax.psum((part_query, part_key, part_value, row_squares), 'kv')  64.9 us
    psum x1, blocking collectives, body(): lax.psum((part_query, part_key, part_value, row_squares), 'kv')  43.6 us
    unnamed x24, local copies, waits for them, and re-layouts  25.9 us
    add x15, other arithmetic, combine(): summed_early * factor_early[..., None]  21.7 us
    all_gather x1, waiting for transfers between devices, merged_2(): everything = jax.tree.map(lambda part: lax.all_gather(part, axis), array)  14.2 us
  transfers between devices with their start and end apart: 3, of which 2 were waited for; matrix products, arithmetic and copies ran while one was open for 13% of the time, Pallas kernels for 0%

commit v1 on v0

v1 whole, which is shorter than its diff:
```python
import functools

import jax
import jax.numpy as jnp
from jax import lax
from jax.experimental import pallas as pl
from jax.experimental.pallas import tpu as pltpu
from jax.sharding import PartitionSpec as P

epsilon = 1e-06
masked_score = -1e30
head_scale = 0.8
stat_rows = 8

VMEM = pl.BlockSpec(memory_space=pltpu.VMEM)
SMEM = pl.BlockSpec(memory_space=pltpu.SMEM)
HBM = pl.BlockSpec(memory_space=pltpu.HBM)
ANY = pl.BlockSpec(memory_space=pl.ANY)
small = pltpu.CompilerParams(vmem_limit_bytes=8 << 20)
large = pltpu.CompilerParams(vmem_limit_bytes=16 << 20)


def in_hbm(array):
    return pltpu.with_memory_space_constraint(array, pltpu.HBM)


def in_vmem(array):
    return pltpu.with_memory_space_constraint(array, pltpu.VMEM)


def pieces(value):
    high = value.astype(jnp.bfloat16).astype(jnp.float32)
    rest = value - high
    middle = rest.astype(jnp.bfloat16).astype(jnp.float32)
    return high, middle, rest - middle


def in_lanes(columns, lanes):
    rows = columns[0].shape[0]
    lane = lax.broadcasted_iota(jnp.int32, (rows, lanes), 1)
    result = jnp.zeros((rows, lanes), jnp.float32)
    for k, column in enumerate(columns):
        result = jnp.where(lane == k, column, result)
    return result


def turned_stats(maximum, totals, dim):
    rows = maximum.shape[0]
    stats = in_lanes(pieces(maximum) + pieces(totals), dim).astype(jnp.bfloat16)
    shape = (stat_rows, dim)
    pick = lax.broadcasted_iota(jnp.int32, shape, 0) == lax.broadcasted_iota(jnp.int32, shape, 1)
    pick = jnp.where(pick, 1.0, 0.0).astype(jnp.bfloat16)
    turned = lax.dot_general(
        pick, stats, (((1,), (1,)), ((), ())), preferred_element_type=jnp.float32
    )
    if rows < dim:
        padding = jnp.zeros((stat_rows, dim - rows), jnp.float32)
        turned = jnp.concatenate([turned, padding], axis=1)
    return turned


def side_by_side(queries, half):
    props, dim = queries[0].shape
    lane = lax.broadcasted_iota(jnp.int32, (props, dim), 1)
    zeros = jnp.zeros((props, dim), queries[0].dtype)
    blocks = []
    for m in range(2):
        for h, query in enumerate(queries):
            kept = jnp.where(lane < half if m == 0 else lane >= half, query, zeros)
            blocks.append(
                jnp.concatenate([kept if k == h else zeros for k in range(len(queries))], axis=1)
            )
    return jnp.concatenate(blocks, axis=0)


def score(queries, keys):
    half = queries[0].shape[1] // 2
    return lax.dot_general(
        side_by_side(queries, half),
        jnp.concatenate(keys, axis=1),
        (((1,), (1,)), ((), ())),
        preferred_element_type=jnp.float32,
    ) * half ** (-0.5)


def soften(masked):
    maximum = jnp.max(masked, axis=1, keepdims=True)
    weight = jnp.exp(masked - maximum)
    totals = jnp.sum(weight, axis=1, keepdims=True)
    return maximum, totals, weight.astype(jnp.bfloat16)


def weigh(weight, values, store):
    dim = values[0].shape[1]
    summed = jnp.dot(weight, jnp.concatenate(values, axis=1), preferred_element_type=jnp.float32)
    count = len(values)
    props = weight.shape[0] // (2 * count)
    for m in range(2):
        for k in range(count):
            first = (m * count + k) * props
            store(first, summed[first : first + props, k * dim : (k + 1) * dim])


def project_kernel(
    tokens_hbm, gain_hbm, w_query, w_key, w_value, out, tokens, gain, held, sems
):
    kv, each, whole = out.shape
    pairs = [(tokens_hbm, tokens), (gain_hbm, gain)]
    pairs += [(w, held.at[k]) for k, w in enumerate((w_query, w_key, w_value))]
    copies = [
        pltpu.make_async_copy(source, target, sems.at[k])
        for k, (source, target) in enumerate(pairs)
    ]
    for copy in copies:
        copy.start()
    copies[0].wait()
    copies[1].wait()
    as_float = tokens[...].astype(jnp.float32)
    squares = jnp.sum(as_float * as_float, axis=1, keepdims=True)
    normed = (as_float * gain[...]).astype(jnp.bfloat16)
    width = w_query.shape[1]
    last = whole - 3 * width
    stats = in_lanes(pieces(squares), last).astype(out.dtype)
    for i in range(kv):
        out[i, :, 3 * width :] = stats[i * each : (i + 1) * each]
    for k, copy in enumerate(copies[2:]):
        copy.wait()
        part = jnp.dot(normed, held[k], preferred_element_type=jnp.float32).astype(out.dtype)
        for i in range(kv):
            out[i, :, k * width : (k + 1) * width] = part[i * each : (i + 1) * each]


def reduce_kernel(features, parts, key_cache, value_cache, out):
    del key_cache, value_cache
    kv = parts.shape[0]
    width = out.shape[2]
    total = parts[0].astype(jnp.float32)
    for k in range(1, kv):
        total = total + parts[k].astype(jnp.float32)
    squares = jnp.sum(total[:, width : width + 3], axis=1, keepdims=True)
    scale = lax.rsqrt(squares / features + epsilon)
    done = (total[:, :width] * scale).astype(out.dtype)
    for k in range(kv):
        out[k] = done


def attend_kernel(
    layout,
    prior,
    accepted,
    qkv,
    keys,
    values,
    message,
    value_out,
    flat,
    scores,
    weights,
    held,
    out_sems,
    cache_sems,
):
    seqs, heads, length, dim = values.shape
    groups = layout.groups()
    leaving = []
    for s in range(seqs // 2):
        copy = pltpu.make_async_copy(values.at[s], value_out.at[s], cache_sems.at[s])
        copy.start()
        leaving.append(copy)
    kv, each = qkv.shape[:2]
    props = kv * each // seqs
    rows = 2 * layout.each * props
    for k in range(kv):
        flat[k * each : (k + 1) * each, :] = qkv[k, :, : heads * dim]
    for at, own in enumerate(groups):
        scores[at] = score(
            [flat[s * props : (s + 1) * props, h * dim : (h + 1) * dim] for s, h in own],
            [keys[s, h] for s, h in own],
        )
    stats = []
    ends = prior[...] + accepted[...] - lax.axis_index("kv") * length
    for at, own in enumerate(groups):
        end = [jnp.broadcast_to(ends[:, s : s + 1], (props, 1)) for s, _ in own]
        end = jnp.concatenate(end * 2, axis=0)
        visible = lax.broadcasted_iota(jnp.int32, (rows, length), 1) < end
        maximum, totals, weight = soften(jnp.where(visible, scores[at], masked_score))
        weights[at] = weight
        stats.append((maximum, totals))
    for at, (maximum, totals) in enumerate(stats):
        held[at, rows:, :] = turned_stats(maximum, totals, dim).astype(held.dtype)
    chunk = len(groups) // out_sems.shape[0]
    for at, own in enumerate(groups):

        def store(first, value, at=at):
            held[at, first : first + props, :] = value.astype(held.dtype)

        weigh(weights[at], [values[s, h] for s, h in own], store)
        if at % chunk == chunk - 1:
            part = pl.ds(at + 1 - chunk, chunk)
            copy = pltpu.make_async_copy(
                held.at[part], message.at[part], out_sems.at[at // chunk]
            )
            copy.start()
            leaving.append(copy)
    for copy in leaving:
        copy.wait()


def tree_kernel(
    layout,
    prior,
    accepted,
    parent,
    lambdas,
    sub_gain,
    qkv,
    key_cache,
    value_cache,
    value_out_in,
    own,
    second,
    key_out,
    value_out,
    flat,
    cached,
    windows,
    read_sems,
    sems,
):
    del value_out_in
    place = lax.axis_index("kv")
    seqs, heads, length, dim = key_cache.shape
    props = parent.shape[1]
    width = heads * dim
    span = 2 * props
    kv, each = qkv.shape[:2]
    reads, starts = [], []
    for s in range(seqs):
        end = prior[s] + accepted[s] - place * length
        start = jnp.clip((end // props) * props, 0, length - span)
        start = pl.multiple_of(start, props)
        starts.append((start, end))
        if s < seqs // 2:
            later = (value_cache.at[s, :, pl.ds(start, span), :], windows.at[s])
        else:
            later = (value_cache.at[s], cached.at[1, s])
        pairs = ((key_cache.at[s], cached.at[0, s]), later)
        for which, (source, target) in enumerate(pairs):
            copy = pltpu.make_async_copy(source, target, read_sems.at[which, s])
            copy.start()
            reads.append(copy)
    for k in range(kv):
        flat[k * each : (k + 1) * each, :] = qkv[k]
    rows = 2 * layout.each * props
    share = second.shape[0] - stat_rows
    split = layout.each * props // share
    mine = [layout.pair(place // split, k) for k in range(layout.each)]
    each = share // layout.each
    for k, (_, h) in enumerate(mine):
        second[k * each : (k + 1) * each, :] = jnp.full((each, dim), lambdas[h], jnp.float32)
    second[share:, :] = jnp.broadcast_to(sub_gain[...] * head_scale, (stat_rows, dim))
    row = lax.broadcasted_iota(jnp.int32, (props, props), 0)
    column = lax.broadcasted_iota(jnp.int32, (props, props), 1)
    reaches = []
    for s, _ in mine:
        above = jnp.full((props, props), -1, jnp.int32)
        for j in range(props):
            above = jnp.where(row == j, parent[s, j], above)
        reach = jnp.where((row == column) | (column == above), 1.0, 0.0)
        steps = 1
        while steps < props:
            now = reach.astype(jnp.bfloat16)
            reach = jnp.dot(now, now, preferred_element_type=jnp.float32)
            reach = jnp.where(reach > 0.5, 1.0, 0.0)
            steps *= 2
        reaches.append(reach)
    visible = jnp.concatenate(reaches * 2, axis=0) > 0.5

    def block(which, s, h):
        tokens = pl.ds(pl.multiple_of(s * props, props), props)
        first = pl.multiple_of(which * width + h * dim, dim)
        return flat[tokens, pl.ds(first, dim)]

    held = {}
    scores = score([block(0, s, h) for s, h in mine], [block(1, s, h) for s, h in mine])
    maximum, totals, weight = soften(jnp.where(visible, scores, masked_score))
    weigh(weight, [block(2, s, h) for s, h in mine], held.__setitem__)
    turned = turned_stats(maximum, totals, dim)
    if split == 1:
        for first, value in held.items():
            own[first : first + props, :] = value
        own[rows:, :] = turned
    else:
        part = place % split
        for k in range(split):

            @pl.when(part == k)
            def _(k=k):
                for m in range(2):
                    first = k * share
                    own[m * share : (m + 1) * share, :] = held[m * props][first : first + share]
                lanes = [turned[:, m * props + k * share :][:, :share] for m in range(2)]
                lanes.append(jnp.zeros((stat_rows, dim - 2 * share), jnp.float32))
                own[2 * share :, :] = jnp.concatenate(lanes, axis=1)

    writes = []
    for s in range(seqs):
        start, end = starts[s]
        offset = lax.broadcasted_iota(jnp.int32, (span, props), 0) + (start - end)
        hot = offset == lax.broadcasted_iota(jnp.int32, (span, props), 1)
        hot = jnp.where(hot, 1.0, 0.0).astype(jnp.bfloat16)
        offset = lax.broadcasted_iota(jnp.int32, (span, dim), 0) + (start - end)
        inside = (offset >= 0) & (offset < props)
        window = pl.ds(start, span)
        if s < seqs // 2:
            later = (windows.at[s], value_out.at[s, :, window, :])
        else:
            later = (cached.at[1, s], value_out.at[s])
        pairs = ((cached.at[0, s], key_out.at[s]), later)
        for which, (source, target) in enumerate(pairs):
            first = (1 + which) * width
            placed = jnp.dot(
                hot,
                flat[s * props : (s + 1) * props, first : first + width],
                preferred_element_type=jnp.float32,
            )
            reads[2 * s + which].wait()
            for h in range(heads):
                new = placed[:, h * dim : (h + 1) * dim]
                if which == 0 or s >= seqs // 2:
                    old = cached[which, s, h, window, :].astype(jnp.float32)
                    cached[which, s, h, window, :] = jnp.where(inside, new, old).astype(
                        cached.dtype
                    )
                else:
                    old = windows[s, h].astype(jnp.float32)
                    windows[s, h] = jnp.where(inside, new, old).astype(windows.dtype)
            copy = pltpu.make_async_copy(source, target, sems.at[which, s])
            copy.start()
            writes.append(copy)
    for copy in writes:
        copy.wait()


def merge_kernel(own, second, message, *rest):
    out = rest[-1]
    kv, rows, dim = message.shape
    count = own.shape[0] // 2 - stat_rows // 2
    both = 2 * count
    stats = message[:, both:, :].astype(jnp.float32)
    maximum = stats[:, 0:1, :] + stats[:, 1:2, :] + stats[:, 2:3, :]
    totals = stats[:, 3:4, :] + stats[:, 4:5, :] + stats[:, 5:6, :]
    stats = own[both:, :]
    own_maximum = stats[0:1, :] + stats[1:2, :] + stats[2:3, :]
    own_totals = stats[3:4, :] + stats[4:5, :] + stats[5:6, :]
    top = jnp.maximum(jnp.max(maximum, axis=0), own_maximum)
    factor = jnp.exp(maximum - top[None])
    own_factor = jnp.exp(own_maximum - top)
    whole = jnp.sum(totals * factor, axis=0) + own_totals * own_factor
    share = jnp.concatenate([(factor / whole[None]).reshape(kv, dim), own_factor / whole], axis=0)
    share = share.T
    summed = own[:both, :] * share[:both, kv : kv + 1]
    for k in range(kv):
        summed = summed + message[k, :both, :].astype(jnp.float32) * share[:both, k : k + 1]
    head_out = summed[:count] - second[:count, :] * summed[count:]
    mean_square = jnp.mean(head_out * head_out, axis=1, keepdims=True)
    attended = head_out * lax.rsqrt(mean_square + epsilon) * second[count : count + 1, :]
    attended = attended.astype(out.dtype)
    blocks, each = out.shape[:2]
    for k in range(blocks):
        first = k % (count // each) * each
        out[k] = attended[first : first + each]


def output_kernel(attended, w_out, out, held):
    seqs, heads, props, dim = attended.shape
    whole = jnp.concatenate(
        [
            jnp.concatenate([attended[s, h] for h in range(heads)], axis=1)
            for s in range(seqs)
        ],
        axis=0,
    )
    held[...] = jnp.dot(whole, w_out[...], preferred_element_type=jnp.float32).astype(out.dtype)
    parts, each = out.shape[:2]
    for k in range(parts):
        first = lax.rem(lax.axis_index("tp") + k, parts) * each
        out[k] = held[pl.ds(pl.multiple_of(first, each), each), :]


def mix_kernel(attended, *rest):
    weights, out = rest[:-1], rest[-1]
    tp = len(weights)
    heads = weights[0].shape[0] // attended.shape[2]
    total = None
    for k, weight in enumerate(weights):
        group = lax.rem(lax.axis_index("tp") + tp - k, tp)
        rows = []
        for s in range(attended.shape[0] // (tp * heads)):
            blocks = [attended[(s * heads + h) * tp + group] for h in range(heads)]
            rows.append(jnp.concatenate(blocks, axis=1))
        part = jnp.dot(
            jnp.concatenate(rows, axis=0), weight[...], preferred_element_type=jnp.float32
        )
        part = part.astype(out.dtype).astype(jnp.float32)
        total = part if total is None else total + part
    out[...] = total.astype(out.dtype)


class Layout:
    def __init__(self, seqs, heads, each, group_step, step):
        self.seqs, self.heads, self.each = seqs, heads, each
        self.group_step, self.step = group_step, step

    def pair(self, group, k):
        index = group * self.group_step + k * self.step
        return index // self.heads, index % self.heads

    def groups(self):
        count = self.seqs * self.heads // self.each
        return [[self.pair(g, k) for k in range(self.each)] for g in range(count)]


def row_of(vector):
    return vector.reshape(1, vector.shape[0])


def exchange(array, axes="kv"):
    return lax.all_to_all(array, axes, 0, 0)


def body(
    tokens,
    norm_gain,
    w_query,
    w_key,
    w_value,
    w_out,
    lambdas,
    sub_gain,
    key_cache,
    value_cache,
    prior,
    accepted,
    parent,
):
    kv, tp = lax.axis_size("kv"), lax.axis_size("tp")
    seqs, props = parent.shape
    heads = lambdas.shape[0]
    length, dim = key_cache.shape[2:]
    count, features = tokens.shape
    width = 3 * heads * dim
    bf16 = jnp.bfloat16

    parts = pl.pallas_call(
        project_kernel,
        out_shape=jax.ShapeDtypeStruct((kv, count // kv, width + dim), bf16),
        in_specs=[HBM] * 5,
        out_specs=VMEM,
        scratch_shapes=[
            pltpu.VMEM(tokens.shape, bf16),
            pltpu.VMEM((1, features), jnp.float32),
            pltpu.VMEM((3,) + w_query.shape, bf16),
            pltpu.SemaphoreType.DMA((5,)),
        ],
        compiler_params=small,
    )(*map(in_hbm, (tokens, row_of(norm_gain), w_query, w_key, w_value)))
    parts = exchange(parts)
    reduced = pl.pallas_call(
        functools.partial(reduce_kernel, features * kv),
        out_shape=jax.ShapeDtypeStruct((kv, count // kv, width), bf16),
        in_specs=[VMEM] + [HBM] * 2,
        out_specs=VMEM,
        compiler_params=small,
    )(parts, in_hbm(key_cache), in_hbm(value_cache))
    qkv = exchange(reduced)

    share = seqs * heads * props // kv
    heads_each = max(1, share // props)
    groups = seqs * heads // heads_each
    rows = 2 * heads_each * props
    by_tokens = heads_each == tp and share == tp * props and seqs % tp == 0
    if by_tokens:
        layout = Layout(seqs, heads, heads_each, 1, groups)
    else:
        layout = Layout(seqs, heads, heads_each, heads_each, 1)

    cache = pltpu.HBM(key_cache.shape, key_cache.dtype)
    message, value_out = pl.pallas_call(
        functools.partial(attend_kernel, layout),
        out_shape=(pltpu.HBM((groups, rows + stat_rows, dim), bf16), cache),
        in_specs=[VMEM] * 5,
        out_specs=(HBM, HBM),
        scratch_shapes=[
            pltpu.VMEM((count, width // 3), bf16),
            pltpu.VMEM((groups, rows, length), jnp.float32),
            pltpu.VMEM((groups, rows, length), bf16),
            pltpu.VMEM((groups, rows + stat_rows, dim), bf16),
            pltpu.SemaphoreType.DMA((4 if groups % 4 == 0 else 1,)),
            pltpu.SemaphoreType.DMA((seqs,)),
        ],
        compiler_params=small,
    )(row_of(prior), row_of(accepted), qkv, in_vmem(key_cache), in_vmem(value_cache))
    if share < props:
        split = props // share
        summed = message[:, :rows].reshape(groups, 2, split, share, dim)
        summed = summed.transpose(0, 2, 1, 3, 4).reshape(kv, 2 * share, dim)
        stats = message[:, rows:, :rows].reshape(groups, stat_rows, 2, split, share)
        stats = stats.transpose(0, 3, 1, 2, 4).reshape(kv, stat_rows, 2 * share)
        stats = jnp.pad(stats, ((0, 0), (0, 0), (0, dim - 2 * share)))
        message = jnp.concatenate([summed, stats], axis=1)
    message = exchange(message)
    own, second, key_out, value_out = pl.pallas_call(
        functools.partial(tree_kernel, layout),
        out_shape=(
            jax.ShapeDtypeStruct((2 * share + stat_rows, dim), jnp.float32),
            jax.ShapeDtypeStruct((share + stat_rows, dim), jnp.float32),
            cache,
            cache,
        ),
        in_specs=[SMEM] * 4 + [VMEM] * 2 + [HBM] * 3,
        out_specs=(VMEM, VMEM, HBM, HBM),
        scratch_shapes=[
            pltpu.VMEM((count, width), bf16),
            pltpu.VMEM((2,) + key_cache.shape, key_cache.dtype),
            pltpu.VMEM((seqs, heads, 2 * props, dim), bf16),
            pltpu.SemaphoreType.DMA((2, seqs)),
            pltpu.SemaphoreType.DMA((2, seqs)),
        ],
        input_output_aliases={8: 3},
        compiler_params=large,
    )(
        prior,
        accepted,
        parent,
        lambdas,
        row_of(sub_gain),
        qkv,
        *map(in_hbm, (key_cache, value_cache, value_out)),
    )
    blocks = (kv * tp, props, dim) if by_tokens else (kv, share, dim)
    columns = w_out.shape[1]
    rings = [[(i, (i + k) % tp) for i in range(tp)] for k in range(1, tp)]
    weights = [lax.ppermute(w_out, "tp", ring) for ring in rings] if by_tokens else []
    attended = pl.pallas_call(
        merge_kernel,
        out_shape=jax.ShapeDtypeStruct(blocks, bf16),
        in_specs=[VMEM] * 3 + [ANY] * len(weights),
        out_specs=VMEM,
        compiler_params=small,
    )(own, second, message, *weights)
    if by_tokens:
        mixed = pl.pallas_call(
            mix_kernel,
            out_shape=jax.ShapeDtypeStruct((count // tp, columns), bf16),
            in_specs=[VMEM] * (1 + tp),
            out_specs=VMEM,
            compiler_params=small,
        )(exchange(attended, ("kv", "tp")), w_out, *weights)
        return (mixed, key_out, value_out)
    partial_value = pl.pallas_call(
        output_kernel,
        out_shape=jax.ShapeDtypeStruct((tp, count // tp, columns), bf16),
        in_specs=[VMEM] * 2,
        out_specs=VMEM,
        scratch_shapes=[pltpu.VMEM((count, columns), bf16)],
        compiler_params=small,
    )(exchange(attended).reshape(seqs, heads, props, dim), w_out)
    mixed = partial_value[0].astype(jnp.float32)
    for k, ring in enumerate(rings):
        mixed = mixed + lax.ppermute(partial_value[k + 1], "tp", ring).astype(jnp.float32)
    return (mixed.astype(bf16), key_out, value_out)


def solution(mesh):
    return jax.shard_map(
        body,
        mesh=mesh,
        in_specs=(
            P(None, "kv"),
            P("kv"),
            P("kv", "tp"),
            P("kv", "tp"),
            P("kv", "tp"),
            P("tp", "kv"),
            P("tp"),
            P(),
            P(None, "tp", "kv", None),
            P(None, "tp", "kv", None),
            P(),
            P(),
            P(),
        ),
        out_specs=(P("tp", "kv"), P(None, "tp", "kv", None), P(None, "tp", "kv", None)),
        check_vma=False,
    )
```

time: 309 us -> 68.8 us (0.22)
  blocking collectives: 133 us -> 47.9 us
  waiting for transfers between devices: 79.2 us -> 2.9 us
  local copies, waits for them, and re-layouts: 27.6 us -> 0.04 us
  matrix products: 26.5 us -> 0 us
  other arithmetic: 25.2 us -> 0 us
  between operations: 14 us -> 0.78 us
  Pallas kernels: 0 us -> 13.2 us
  starting transfers between devices: 0.12 us -> 3.72 us
    all_gather x2 -> x0, blocking collectives: 89.4 us -> none  [merged_2(): everything = jax.tree.map(lambda part: lax.all_gather(part, axis), array)]
    psum x1 -> x0, waiting for transfers between devices: 64.9 us -> none  [body(): lax.psum((part_query, part_key, part_value, row_squares), 'kv')]
    all_to_all x0 -> x3, blocking collectives: none -> 47.9 us  [exchange(): return lax.all_to_all(array, axes, 0, 0)]
    psum x1 -> x0, blocking collectives: 43.6 us -> none  [body(): lax.psum((part_query, part_key, part_value, row_squares), 'kv')]
    dot_general x26 -> x0, matrix products: 26.5 us -> none  [the longest x1 5.51 us: body(): jnp.einsum('spj,shjc->shpc', hot_rows, new_key, preferred_element_type=jn...]
    unnamed x24 -> x16, local copies, waits for them, and re-layouts: 25.9 us -> 0.04 us
    add x33 -> x0, other arithmetic: 22.3 us -> none  [the longest x15 21.7 us: combine(): summed_early * factor_early[..., None]]
    all_gather x1 -> x0, waiting for transfers between devices: 14.2 us -> none  [merged_2(): everything = jax.tree.map(lambda part: lax.all_gather(part, axis), array)]
  transfers between devices with their start and end apart: 3 -> 2, of which waited for: 2 -> 1; matrix products, arithmetic and copies ran while one was open for 13% -> 0% of each run, Pallas kernels for 0% -> 10%
where the time goes in v1:
time: 68.8 us; the launch traced here: 68.5 us
  blocking collectives  47.9 us (70%)
  Pallas kernels  13.2 us (19%)
  starting transfers between devices  3.72 us (5%)
  waiting for transfers between devices  2.9 us (4%)
  between operations  0.78 us (1%)
    all_to_all x3, blocking collectives, exchange(): return lax.all_to_all(array, axes, 0, 0)  47.9 us
    pallas_call x1, Pallas kernels, body(): pl.pallas_call(functools.partial(tree_kernel, layout), out_shape=(jax.Sha...  6.7 us
    all_to_all x1, starting transfers between devices, exchange(): return lax.all_to_all(array, axes, 0, 0)  3.64 us
    pallas_call x1, Pallas kernels, body(): pl.pallas_call(functools.partial(attend_kernel, layout), out_shape=(pltpu...  3.21 us
    all_to_all x1, waiting for transfers between devices, exchange(): return lax.all_to_all(array, axes, 0, 0)  2.89 us
    pallas_call x1, Pallas kernels, body(): pl.pallas_call(project_kernel, out_shape=jax.ShapeDtypeStruct((kv, count...  1.76 us
  transfers between devices with their start and end apart: 2, of which 1 were waited for; matrix products, arithmetic and copies ran while one was open for 0% of the time, Pallas kernels for 10%

profile of v1, /device:TPU:0, one launch (start us, length us, event | category | flops | bytes accessed | tf_op | source)
XLA Modules:
  0.0 68.5 jit_solution(12729657666269212337)
XLA Ops:
  0.6 1.8 %shard_map.148 = bf16[16,4,3200]{2,1,0:T(4,128)(2,1)S(1)} custom-call(bf16[64,256]{1,0:T(8,128)(2,1)} %tokens_hbm.1, f32[1,256]{1,0:T(1,128)} %bitcast.7, bf16[256,1024]{1,0:T(8,128)(2,1)} %w_query.1, bf16[256,1024]{1,0:T(8,128)(2,1)} %w_key.1, bf16[256,1024]{1,0:T(8,128)(2,1)} %w_value.1), custom_call_target="tpu_custom_call" | custom-call | tf_op jit(solution)/shard_map/pallas_call | solution.py:455
  2.4 21.1 %all_to_all.20.parts = bf16[16,4,3200]{2,1,0:T(4,128)(2,1)S(1)} all-to-all(bf16[16,4,3200]{2,1,0:T(4,128)(2,1)S(1)} %shard_map.148), channel_id=1, replica_groups=mesh['kv'=16,'tp'=2] {'kv'}, dimensions={0} | all-to-all | bytes 819200 | tf_op jit(solution)/shard_map/all_to_all | solution.py:429
  23.5 0.0 copy-start
  23.5 0.0 copy-start.1
  23.5 0.0 copy-start.4
  23.5 0.0 copy-start.5
  23.5 0.1 shard_map.149
  23.6 15.7 %all_to_all.21.qkv = bf16[16,4,3072]{2,1,0:T(4,128)(2,1)S(1)} all-to-all(bf16[16,4,3072]{2,1,0:T(4,128)(2,1)S(1)} %shard_map.149), channel_id=1, replica_groups=mesh['kv'=16,'tp'=2] {'kv'}, dimensions={0} | all-to-all | bytes 786432 | tf_op jit(solution)/shard_map/all_to_all | solution.py:429
  39.3 0.0 copy-done
  39.3 0.0 copy-done.1
  39.4 0.0 copy-done.4
  39.4 0.0 copy-done.5
  39.4 0.0 copy-start.2
  39.4 0.0 copy-start.3
  39.4 0.0 copy-start.6
  39.4 0.0 copy-start.7
  39.4 3.2 %shard_map.150 = (bf16[16,72,128]{2,1,0:T(8,128)(2,1)}, bf16[4,8,512,128]{3,2,1,0:T(8,128)(2,1)}) custom-call(s32[1,4]{1,0:T(1,128)S(1)} %bitcast.4, s32[1,4]{1,0:T(1,128)S(1)} %bitcast.5, bf16[16,4,3072]{2,1,0:T(4,128)(2,1)S(1)} %all_to_all.21.qkv, bf16[4,8,512,128]{3,2,1,0:T(8,128)(2,1)S(1)} %copy-done, bf16[4,8,512,128]{3,2,1,0:T(8,128)(2,1)S(1)} %copy-done.1), custom_call_target="tpu_custom_call" | custom-call | tf_op jit(solution)/shard_map/pallas_call | solution.py:489
  42.6 3.6 %all-to-all-start.2 = ((bf16[16,72,128]{2,1,0:T(8,128)(2,1)}), bf16[16,72,128]{2,1,0:T(8,128)(2,1)S(1)}, u32[]{:S(2)}, u32[]{:S(2)}) async-start(bf16[16,72,128]{2,1,0:T(8,128)(2,1)} %get-tuple-element.12), calls=%async_computation.2 | async-start | bytes 589824 | tf_op jit(solution)/shard_map/all_to_all | solution.py:429
  46.3 0.0 copy-done.2
  46.3 0.1 collective-permute-start
  46.4 0.0 copy-done.3
  46.4 0.0 copy-done.6
  46.4 0.0 copy-done.7
  46.4 6.7 %shard_map.151 = (f32[72,128]{1,0:T(8,128)S(1)}, f32[40,128]{1,0:T(8,128)S(1)}, bf16[4,8,512,128]{3,2,1,0:T(8,128)(2,1)}, bf16[4,8,512,128]{3,2,1,0:T(8,128)(2,1)}) custom-call(s32[4]{0:T(128)S(1)} %copy-done.4, s32[4]{0:T(128)S(1)} %copy-done.5, s32[4,16]{1,0:T(4,128)S(1)} %copy-done.3, f32[8]{0:T(128)S(1)} %copy-done.6, ...), custom_call_target="tpu_custom_call", output_to_operand_aliasing={{3}: (8, {})} | custom-call | tf_op jit(solution)/shard_map/pallas_call | solution.py:513
  53.1 0.0 collective-permute-done.rest_0_.rest_1_
  53.1 2.9 %all-to-all-done.2.message = bf16[16,72,128]{2,1,0:T(8,128)(2,1)S(1)} async-done(((bf16[16,72,128]{2,1,0:T(8,128)(2,1)}), bf16[16,72,128]{2,1,0:T(8,128)(2,1)S(1)}, u32[]{:S(2)}, u32[]{:S(2)}) %all-to-all-start.2) | async-done | bytes 294944 | tf_op jit(solution)/shard_map/all_to_all | solution.py:429
  56.0 0.5 shard_map.152
  56.5 11.1 %all_to_all.22.attended = bf16[32,16,128]{2,1,0:T(8,128)(2,1)S(1)} all-to-all(bf16[32,16,128]{2,1,0:T(8,128)(2,1)S(1)} %shard_map.152), channel_id=1, replica_groups=mesh['kv'=16,'tp'=2] {'kv','tp'}, dimensions={0} | all-to-all | bytes 262144 | tf_op jit(solution)/shard_map/all_to_all | solution.py:429
  67.6 0.9 %shard_map.153 = bf16[32,256]{1,0:T(8,128)(2,1)} custom-call(bf16[32,16,128]{2,1,0:T(8,128)(2,1)S(1)} %all_to_all.22.attended, bf16[1024,256]{1,0:T(8,128)(2,1)S(1)} %copy-done.2, bf16[1024,256]{1,0:T(8,128)(2,1)S(1)} %collective-permute-done.rest_0_.rest_1_), custom_call_target="tpu_custom_call" | custom-call | tf_op jit(solution)/shard_map/pallas_call | solution.py:553
Async XLA Ops:
  23.5 15.9 %copy-start = (bf16[4,8,512,128]{3,2,1,0:T(8,128)(2,1)S(1)}, bf16[4,8,512,128]{3,2,1,0:T(8,128)(2,1)}, u32[]{:S(2)}) copy-start(bf16[4,8,512,128]{3,2,1,0:T(8,128)(2,1)} %key_cache.3) | copy-start | bytes 12582916
  23.5 15.9 %copy-start.1 = (bf16[4,8,512,128]{3,2,1,0:T(8,128)(2,1)S(1)}, bf16[4,8,512,128]{3,2,1,0:T(8,128)(2,1)}, u32[]{:S(2)}) copy-start(bf16[4,8,512,128]{3,2,1,0:T(8,128)(2,1)} %value_cache.3) | copy-start | bytes 12582916
  23.5 15.9 %copy-start.4 = (s32[4]{0:T(128)S(1)}, s32[4]{0:T(128)}, u32[]{:S(2)}) copy-start(s32[4]{0:T(128)} %prior.1) | copy-start | bytes 52
  23.5 15.9 %copy-start.5 = (s32[4]{0:T(128)S(1)}, s32[4]{0:T(128)}, u32[]{:S(2)}) copy-start(s32[4]{0:T(128)} %accepted.1) | copy-start | bytes 52
  39.4 6.9 %copy-start.2 = (bf16[1024,256]{1,0:T(8,128)(2,1)S(1)}, bf16[1024,256]{1,0:T(8,128)(2,1)}, u32[]{:S(2)}) copy-start(bf16[1024,256]{1,0:T(8,128)(2,1)} %rest_0_.1) | copy-start | bytes 1572868
  39.4 7.0 %copy-start.3 = (s32[4,16]{1,0:T(4,128)S(1)}, s32[4,16]{1,0:T(4,128)}, u32[]{:S(2)}) copy-start(s32[4,16]{1,0:T(4,128)} %parent.1) | copy-start | bytes 772
  39.4 7.0 %copy-start.6 = (f32[8]{0:T(128)S(1)}, f32[8]{0:T(128)}, u32[]{:S(2)}) copy-start(f32[8]{0:T(128)} %lambdas.1) | copy-start | bytes 100
  39.4 7.0 %copy-start.7 = (f32[128]{0:T(128)S(1)}, f32[128]{0:T(128)}, u32[]{:S(2)}) copy-start(f32[128]{0:T(128)} %param.20) | copy-start | bytes 1540
  42.6 13.4 %all-to-all-start.2 = ((bf16[16,72,128]{2,1,0:T(8,128)(2,1)}), bf16[16,72,128]{2,1,0:T(8,128)(2,1)S(1)}, u32[]{:S(2)}, u32[]{:S(2)}) async-start(bf16[16,72,128]{2,1,0:T(8,128)(2,1)} %get-tuple-element.12), calls=%async_computation.2 | async-start | bytes 589824 | tf_op jit(solution)/shard_map/all_to_all | solution.py:429
  46.3 6.8 %collective-permute-start = (bf16[1024,256]{1,0:T(8,128)(2,1)S(1)}, bf16[1024,256]{1,0:T(8,128)(2,1)S(1)}, u32[]{:S(2)}, u32[]{:S(2)}) collective-permute-start(bf16[1024,256]{1,0:T(8,128)(2,1)S(1)} %copy-done.2), channel_id=1, source_target_pairs={{0,1},{1,0},{2,3},{3,2},{4,5},{5,4},{6,7},{7,6},{8,9},{9,8},{10,11... | collective-permute-start | bytes 1572872 | tf_op jit(solution)/shard_map/ppermute | solution.py:544
